TPU v7x, 32 devices: a whole 2x2x4 slice. The times are simulated.
32 devices in a mesh: sp: 8 (over z, x), tp: 4 (over y, core).
Axes of the slice: x: 2, y: 2, z: 4, core: 2. Of those that a mesh axis runs over, the one named last changes fastest.
Arguments:
- moe_input: bfloat16 [2048, 2048], P('sp'), may hold values from -6 to 6
- cotangent: bfloat16 [2048, 2048], P('sp'), may hold values from -6 to 6
- expert_ids: int32 [2048, 2], P('sp'), may hold values from 0 to 7, as said below
- route_weights: float32 [2048, 2], P('sp'), may hold values from 0.05 to 1
- gate_weight: bfloat16 [8, 2048, 1024], P('sp', None, 'tp'), may hold values from -0.125 to 0.125
- up_weight: bfloat16 [8, 2048, 1024], P('sp', None, 'tp'), may hold values from -0.125 to 0.125
- down_weight: bfloat16 [8, 1024, 2048], P('sp', 'tp'), may hold values from -0.1875 to 0.1875
- out_weight: bfloat16 [2048, 1024], P(None, 'tp'), may hold values from -0.1875 to 0.1875
- mixer_out: bfloat16 [2048, 1024], P('sp', 'tp'), may hold values from -6 to 6
- query_vectors: bfloat16 [2048, 512], P('sp', 'tp'), may hold values from -0.62109375 to 0.62109375
- key_vectors: bfloat16 [2048, 512], P('sp', 'tp'), may hold values from -0.62109375 to 0.62109375
- value_vectors: bfloat16 [2048, 1024], P('sp', 'tp'), may hold values from -6 to 6
- log_decay: float32 [2048, 512], P('sp', 'tp'), may hold values from -2 to 0
Outputs:
- grad_gate: bfloat16 [8, 2048, 1024], P('sp', None, 'tp')
- grad_up: bfloat16 [8, 2048, 1024], P('sp', None, 'tp')
- grad_down: bfloat16 [8, 1024, 2048], P('sp', 'tp')
- grad_out_weight: float32 [2048, 1024], P('sp', 'tp')
- grad_queries: bfloat16 [2048, 512], P('sp', 'tp')
- grad_keys: bfloat16 [2048, 512], P('sp', 'tp')
- grad_values: bfloat16 [2048, 1024], P('sp', 'tp')
- grad_log_decay: float32 [2048, 512], P('sp', 'tp')
Inputs may be any that keep to these rules, and one draw needn't show every extreme that they name: `expert_ids`: each row names two different experts of one group, expert e lying in group e // 2. Each aligned block of 256 rows names every expert exactly 64 times and has equally many rows in each of the 4 groups.
All inputs are finite; a program needn't handle non-finite values.
Results may differ from a plain program's by a relative error of at most 0.01145.
Values may be sent and summed in bfloat16 or wider, within the bound.
A program may use at most 64 MiB of HBM per device.

v0:
```python
import jax
import jax.numpy as jnp
from jax import lax
from jax.sharding import PartitionSpec as P

KEY_CHANNELS = 64
VAL_DIM = 128
BLOCK = 64
HIGHEST = lax.Precision.HIGHEST


def entering(shard, axis, combine, identity, reverse):
    devices, place = (lax.axis_size(axis), lax.axis_index(axis))
    everything = jax.tree.map(lambda part: lax.all_gather(part, axis), shard)
    start = jax.tree.map(
        lambda part, zero: jnp.broadcast_to(jnp.asarray(zero, part.dtype), part.shape),
        shard,
        identity,
    )

    def lap(k, before):
        at = devices - 1 - k if reverse else k
        reached = at > place if reverse else at < place
        new = combine(before, jax.tree.map(lambda part: part[at], everything))
        return jax.tree.map(lambda a, b: jnp.where(reached, a, b), new, before)

    return lax.fori_loop(0, devices, lap, start)


def block_step(memory, inputs):
    query_block, key_block, value_block, decay_block = inputs
    block_len = query_block.shape[1]
    causal = jnp.tril(jnp.ones((block_len, block_len), dtype=bool))
    cumulative = jnp.cumsum(decay_block, axis=1)
    carried = jnp.einsum(
        "hcd,hdv->hcv", query_block * jnp.exp(cumulative), memory, precision=HIGHEST
    )
    difference = cumulative[:, :, None, :] - cumulative[:, None, :, :]
    decay = jnp.exp(jnp.where(causal[None, :, :, None], difference, -jnp.inf))
    scores = jnp.einsum("htd,hsd,htsd->hts", query_block, key_block, decay, precision=HIGHEST)
    within = jnp.einsum("hts,hsv->htv", scores, value_block, precision=HIGHEST)
    final_row = cumulative[:, -1:, :]
    memory = jnp.exp(final_row[:, 0, :])[:, :, None] * memory + jnp.einsum(
        "hsd,hsv->hdv", key_block * jnp.exp(final_row - cumulative), value_block, precision=HIGHEST
    )
    return (memory, carried + within)


def run_blocks(query_heads, key_heads, value_heads, decay_heads, memory):
    head_count = query_heads.shape[0]
    length = query_heads.shape[1]
    block_count = length // BLOCK

    def to_blocks(matrix):
        return matrix.reshape(head_count, block_count, BLOCK, matrix.shape[-1]).transpose(
            1, 0, 2, 3
        )

    memory, outputs = lax.scan(
        jax.checkpoint(block_step),
        memory,
        (
            to_blocks(query_heads),
            to_blocks(key_heads),
            to_blocks(value_heads),
            to_blocks(decay_heads),
        ),
    )
    return (outputs.transpose(1, 0, 2, 3).reshape(head_count, length, outputs.shape[-1]), memory)


def chain_combine(former, latter):
    return (former[0] * latter[0], latter[1] + latter[0][:, :, None] * former[1])


def expert_pass(routed, routed_cot, gate_local, up_local, down_local):
    pre_gate = jnp.dot(routed, gate_local, preferred_element_type=jnp.float32)
    pre_up = jnp.dot(routed, up_local, preferred_element_type=jnp.float32)
    sigmoid_gate = jax.nn.sigmoid(pre_gate)
    activated = pre_gate * sigmoid_gate
    hidden = (activated * pre_up).astype(jnp.bfloat16)
    delta_hidden = jnp.dot(routed_cot, down_local.T, preferred_element_type=jnp.float32)
    grad_down = jnp.dot(hidden.T, routed_cot, preferred_element_type=jnp.float32).astype(
        jnp.bfloat16
    )
    delta_gate = (
        delta_hidden * pre_up * sigmoid_gate * (1.0 + pre_gate * (1.0 - sigmoid_gate))
    ).astype(jnp.bfloat16)
    delta_up = (delta_hidden * activated).astype(jnp.bfloat16)
    grad_gate = jnp.dot(routed.T, delta_gate, preferred_element_type=jnp.float32).astype(
        jnp.bfloat16
    )
    grad_up = jnp.dot(routed.T, delta_up, preferred_element_type=jnp.float32).astype(jnp.bfloat16)
    partial_value = jnp.dot(delta_gate, gate_local.T, preferred_element_type=jnp.float32)
    partial_value = partial_value + jnp.dot(
        delta_up, up_local.T, preferred_element_type=jnp.float32
    )
    return (grad_gate, grad_up, grad_down, partial_value)


def mixer_backward(query_vectors, key_vectors, value_vectors, log_decay, delta_mixer):
    tok_count = query_vectors.shape[0]

    def heads_first(matrix, channel_size):
        return matrix.astype(jnp.float32).reshape(tok_count, -1, channel_size).transpose(1, 0, 2)

    def tokens_first(matrix):
        return matrix.transpose(1, 0, 2).reshape(tok_count, -1)

    query_heads = heads_first(query_vectors, KEY_CHANNELS)
    key_heads = heads_first(key_vectors, KEY_CHANNELS)
    value_heads = heads_first(value_vectors, VAL_DIM)
    decay_heads = heads_first(log_decay, KEY_CHANNELS)
    cot_heads = heads_first(delta_mixer, VAL_DIM)
    cumulative = jnp.cumsum(decay_heads, axis=1)
    decay_total = cumulative[:, -1, :]
    retention = jnp.exp(decay_total)
    local_state = jnp.einsum(
        "hld,hlv->hdv",
        key_heads * jnp.exp(decay_total[:, None, :] - cumulative),
        value_heads,
        precision=HIGHEST,
    )
    local_pull = jnp.einsum(
        "hld,hlv->hdv",
        query_heads * KEY_CHANNELS ** (-0.5) * jnp.exp(cumulative),
        cot_heads,
        precision=HIGHEST,
    )
    identity = (jnp.ones_like(retention), jnp.zeros_like(local_state))
    start_state = entering((retention, local_state), "sp", chain_combine, identity, False)[1]
    end_pull = entering((retention, local_pull), "sp", chain_combine, identity, True)[1]

    def local_forward(query_in, key_in, value_in, decay_in):
        return run_blocks(
            query_in * KEY_CHANNELS ** (-0.5), key_in, value_in, decay_in, start_state
        )

    pullback = jax.vjp(local_forward, query_heads, key_heads, value_heads, decay_heads)[1]
    grads = pullback((cot_heads, end_pull))
    return (
        tokens_first(grads[0]).astype(jnp.bfloat16),
        tokens_first(grads[1]).astype(jnp.bfloat16),
        tokens_first(grads[2]).astype(jnp.bfloat16),
        tokens_first(grads[3]),
    )


def shards(
    moe_input,
    cotangent,
    expert_ids,
    route_weights,
    gate_weight,
    up_weight,
    down_weight,
    out_weight,
    mixer_out,
    query_vectors,
    key_vectors,
    value_vectors,
    log_decay,
):
    tok_count = moe_input.shape[0]
    model_width = moe_input.shape[1]
    slot_total = 2 * tok_count
    flat_ids = expert_ids.reshape(-1)
    sorting = jnp.argsort(flat_ids, stable=True)
    source_rows = sorting // 2
    inverse = jnp.argsort(sorting)
    gate_local = gate_weight[0]
    up_local = up_weight[0]
    down_local = down_weight[0]
    quarter = model_width // lax.axis_size("tp")
    offset = lax.axis_index("tp") * quarter
    own_input = lax.dynamic_slice_in_dim(moe_input, offset, quarter, 1)
    own_cot = lax.dynamic_slice_in_dim(cotangent, offset, quarter, 1)
    own_scaled = (route_weights[:, :, None] * own_cot[:, None, :].astype(jnp.float32)).astype(
        jnp.bfloat16
    )
    own_scaled = own_scaled.reshape(slot_total, quarter)
    arrived = (
        lax.all_to_all(own_input[source_rows], "sp", split_axis=0, concat_axis=0, tiled=True),
        lax.all_to_all(own_scaled[sorting], "sp", split_axis=0, concat_axis=0, tiled=True),
    )
    routed, routed_cot = (
        lax.all_gather(arrived[0], "tp", axis=1, tiled=True),
        lax.all_gather(arrived[1], "tp", axis=1, tiled=True),
    )
    grad_gate, grad_up, grad_down, partial_value = expert_pass(
        routed, routed_cot, gate_local, up_local, down_local
    )
    summed = lax.psum_scatter(
        partial_value.astype(jnp.bfloat16), "tp", scatter_dimension=1, tiled=True
    )
    returned = lax.all_to_all(summed, "sp", split_axis=0, concat_axis=0, tiled=True)
    per_slot = returned[inverse].reshape(tok_count, 2, quarter).astype(jnp.float32)
    own_grad = (own_cot.astype(jnp.float32) + per_slot[:, 0] + per_slot[:, 1]).astype(jnp.bfloat16)
    token_grad = lax.all_gather(own_grad, "tp", axis=1, tiled=True)
    delta_mixer = jnp.dot(token_grad, out_weight, preferred_element_type=jnp.float32).astype(
        jnp.bfloat16
    )
    grad_out_weight = lax.psum_scatter(
        jnp.dot(token_grad.T, mixer_out, preferred_element_type=jnp.float32),
        "sp",
        scatter_dimension=0,
        tiled=True,
    )
    gradients = mixer_backward(query_vectors, key_vectors, value_vectors, log_decay, delta_mixer)
    return (
        grad_gate[None],
        grad_up[None],
        grad_down[None],
        grad_out_weight,
        gradients[0],
        gradients[1],
        gradients[2],
        gradients[3],
    )


def solution(mesh):
    return jax.shard_map(
        shards,
        mesh=mesh,
        in_specs=(
            P("sp", None),
            P("sp", None),
            P("sp", None),
            P("sp", None),
            P("sp", None, "tp"),
            P("sp", None, "tp"),
            P("sp", "tp", None),
            P(None, "tp"),
            P("sp", "tp"),
            P("sp", "tp"),
            P("sp", "tp"),
            P("sp", "tp"),
            P("sp", "tp"),
        ),
        out_specs=(
            P("sp", None, "tp"),
            P("sp", None, "tp"),
            P("sp", "tp", None),
            P("sp", "tp"),
            P("sp", "tp"),
            P("sp", "tp"),
            P("sp", "tp"),
            P("sp", "tp"),
        ),
        check_vma=False,
    )
```

profile of v0, /device:TPU:0, one launch (start us, length us, event | category | flops | bytes accessed | tf_op | source)
XLA Modules:
  0.0 286.6 jit_solution(11970388747778692487)
XLA Ops:
  7.2 0.9 copy.179
  8.3 3.8 %sort.34 = (s32[512]{0:T(512)}, s32[512]{0:T(512)S(1)}) sort(s32[512]{0:T(512)S(1)} %reshape.170, s32[512]{0:T(512)S(1)} %iota.42), dimensions={0}, to_apply=%region_0.0 | sort | flops 4608 | bytes 8192 | tf_op jit(solution)/shard_map/jit(argsort)/sort | solution.py:168
  12.1 1.1 dynamic-slice_convert_fusion
  13.2 2.0 gather_fusion
  15.2 21.7 %all_to_all.36 = bf16[8,64,512]{2,1,0:T(8,128)(2,1)} all-to-all(bf16[8,64,512]{2,1,0:T(8,128)(2,1)S(1)} %bitcast.315), channel_id=1, replica_groups=mesh['sp'=8,'tp'=4] {'sp'}, dimensions={0} | all-to-all | bytes 1048576 | tf_op jit(solution)/shard_map/all_to_all | solution.py:183
  37.3 0.7 mul.256
  38.5 2.0 gather_fusion.1
  40.5 17.8 %all_to_all.37 = bf16[8,64,512]{2,1,0:T(8,128)(2,1)} all-to-all(bf16[8,64,512]{2,1,0:T(8,128)(2,1)S(1)} %bitcast.316), channel_id=1, replica_groups=mesh['sp'=8,'tp'=4] {'sp'}, dimensions={0} | all-to-all | bytes 1048576 | tf_op jit(solution)/shard_map/all_to_all | solution.py:184
  58.7 2.3 fusion.32
  61.0 2.5 fusion.35
  63.5 19.3 %all-gather.9.cloned.1.call-done = bf16[512,2048]{1,0:T(8,128)(2,1)} async-done(((bf16[512,512]{1,0:T(8,128)(2,1)}), bf16[512,2048]{1,0:T(8,128)(2,1)}) %all-gather.9.cloned.1.call-update) | async-done | bytes 2097168 | tf_op jit(solution)/shard_map/all_gather | solution.py:188
  82.8 2.7 multiply_convert_fusion.2
  85.5 0.7 copy-done.12
  86.2 0.7 fusion.30
  87.0 2.1 add_convert_fusion
  89.5 1.2 reduce-window.6
  91.7 20.5 %all-gather.1 = f32[16,1,64]{2,1,0:T(1,128)S(1)} all-gather(f32[2,1,64]{2,1,0:T(1,128)S(1)} %bitcast.346), channel_id=3, replica_groups=mesh['sp'=8,'tp'=4] {'sp'}, dimensions={0}, use_global_device_ids=true | all-gather | bytes 4608 | tf_op jit(solution)/shard_map/all_gather | solution.py:14
  112.9 31.5 %all-gather.2 = f32[16,64,128]{2,1,0:T(8,128)S(1)} all-gather(f32[2,64,128]{2,1,0:T(8,128)S(1)} %fusion.43), channel_id=4, replica_groups=mesh['sp'=8,'tp'=4] {'sp'}, dimensions={0}, use_global_device_ids=true | all-gather | bytes 589824 | tf_op jit(solution)/shard_map/all_gather | solution.py:14
  144.5 3.5 %all-to-all-start.2 = ((bf16[8,64,512]{2,1,0:T(8,128)(2,1)}), bf16[8,64,512]{2,1,0:T(8,128)(2,1)S(1)}, u32[]{:S(2)}, u32[]{:S(2)}) async-start(bf16[8,64,512]{2,1,0:T(8,128)(2,1)} %bitcast.335), calls=%async_computation.3 | async-start | bytes 1048576 | tf_op jit(solution)/shard_map/all_to_all | solution.py:196
  148.2 1.1 while.67
  149.5 3.8 %sort.35 = (s32[512]{0:T(512)}, s32[512]{0:T(512)S(1)}) sort(s32[512]{0:T(512)S(1)} %get-tuple-element.514, s32[512]{0:T(512)S(1)} %iota.43), dimensions={0}, to_apply=%region_2.3 | sort | flops 4608 | bytes 8192 | tf_op jit(solution)/shard_map/jit(argsort)/sort | solution.py:170
  153.8 4.4 %all-to-all-done.2 = bf16[8,64,512]{2,1,0:T(8,128)(2,1)S(1)} async-done(((bf16[8,64,512]{2,1,0:T(8,128)(2,1)}), bf16[8,64,512]{2,1,0:T(8,128)(2,1)S(1)}, u32[]{:S(2)}, u32[]{:S(2)}) %all-to-all-start.2) | async-done | bytes 524320 | tf_op jit(solution)/shard_map/all_to_all | solution.py:196
  158.2 2.6 gather_fusion.2
  160.8 1.7 reshape.184
  162.5 0.8 fusion.53
  163.3 1.9 fusion.40
  165.2 5.1 %while.64 = (s32[]{:T(128)}, f32[2,64,128]{2,1,0:T(8,128)S(1)}, f32[4,2,64,128]{3,2,1,0:T(8,128)}, f32[4,2,64,64]{3,2,1,0:T(8,128)S(1)}, f32[4,2,64,64]{2,0,3,1:...) while((s32[]{:T(128)}, f32[2,64,128]{2,1,0:T(8,128)S(1)}, ...), condition=%wide.region_12.13_spmd, body=%wide.region_10.12_spmd.sunk | while | flops 13148162 | bytes 725105 | solution.py:59
  165.3 0.6 bitcast_dynamic-update-slice_fusion.5
  167.8 0.6 bitcast_dynamic-update-slice_fusion.5
  169.1 0.6 bitcast_dynamic-update-slice_fusion.5
  170.5 0.7 broadcast_convert_fusion
  171.2 3.4 %fusion.27 = bf16[1,2048,256]{2,1,0:T(8,128)(2,1)} fusion(bf16[512,2048]{1,0:T(8,128)(2,1)} %all-gather.7.cloned.1.call-done, bf16[512,256]{1,0:T(8,128)(2,1)S(1)} %copy-done.13), kind=kOutput, calls=%fused_computation.70 | convolution fusion | flops 537395200 | bytes 3407872 | tf_op jit(solution)/shard_map/dot_general | solution.py:90
  174.6 2.8 fusion.28
  177.4 1.8 fusion.29
  179.2 1.0 all-gather.11.cloned.1.call-done
  180.2 3.2 %fusion.57 = f32[2048,256]{1,0:T(8,128)} fusion(bf16[256,2048]{1,0:T(8,128)(2,1)} %all-gather.11.cloned.1.call-done, bf16[256,256]{1,0:T(8,128)(2,1)} %param.29), kind=kOutput, calls=%fused_computation.131 | convolution fusion | flops 268435456 | bytes 3276800 | tf_op jit(solution)/shard_map/dot_general | solution.py:204
  183.4 2.4 convolution_convert_fusion.3
  185.8 1.0 copy.189
  187.2 32.7 %all-gather = f32[16,64,128]{2,1,0:T(8,128)S(1)} all-gather(f32[2,64,128]{2,1,0:T(8,128)S(1)} %fusion.45), channel_id=2, replica_groups=mesh['sp'=8,'tp'=4] {'sp'}, dimensions={0}, use_global_device_ids=true | all-gather | bytes 589824 | tf_op jit(solution)/shard_map/all_gather | solution.py:14
  219.9 1.2 while.66
  221.2 0.7 broadcast.54.clone
  221.9 52.6 %while.65 = (s32[]{:T(128)}, f32[2,64,128]{2,1,0:T(8,128)S(1)}, f32[4,2,64,64]{3,1,2,0:T(2,128)S(1)}, bf16[4,2,64,64]{3,1,2,0:T(2,128)(2,1)}, bf16[4,2,64,128]{3...) while((s32[]{:T(128)}, f32[2,64,128]{2,1,0:T(8,128)S(1)}, ...), condition=%wide.region_20.21_spmd, body=%wide.region_13.20_spmd.sunk | while | flops 87216128 | bytes 5496629 | solution.py:59
  221.9 0.9 dynamic-slice_bitcast_fusion.14
  224.2 4.1 %fusion.124 = (f32[2,64,64]{2,1,0:T(8,128)S(1)}, f32[2,64,64]{2,1,0:T(8,128)S(1)}, f32[2,64,64]{2,1,0:T(8,128)S(1)}) fusion(f32[2,64,64]{1,2,0:T(8,128)S(1)} %copy.335, f32[2,64,64]{1,2,0:T(8,128)S(1)} %copy.336, f32[2,64,64]{2,1,0:T(8,128)S(1)} %reduce_window_sum.59, f32[2,64,64]{2,1,0:T(8,128)S(1)} %fusion.123, ...), kind=kLoop, calls=%fused_computation.32.clone.1 | loop fusion | flops 5218304 | bytes 233472 | tf_op jit(solution)/shard_map/transpose(jvp())/while/body/eval_jaxpr/checkpoint/reduce_sum | solution.py:38
  229.2 2.0 fusion.131
  231.1 2.0 fusion.132
  235.1 0.9 dynamic-slice_bitcast_fusion.14
  237.3 4.1 %fusion.124 = (f32[2,64,64]{2,1,0:T(8,128)S(1)}, f32[2,64,64]{2,1,0:T(8,128)S(1)}, f32[2,64,64]{2,1,0:T(8,128)S(1)}) fusion(f32[2,64,64]{1,2,0:T(8,128)S(1)} %copy.335, f32[2,64,64]{1,2,0:T(8,128)S(1)} %copy.336, f32[2,64,64]{2,1,0:T(8,128)S(1)} %reduce_window_sum.59, f32[2,64,64]{2,1,0:T(8,128)S(1)} %fusion.123, ...), kind=kLoop, calls=%fused_computation.32.clone.1 | loop fusion | flops 5218304 | bytes 233472 | tf_op jit(solution)/shard_map/transpose(jvp())/while/body/eval_jaxpr/checkpoint/reduce_sum | solution.py:38
  242.3 2.0 fusion.131
  244.3 2.0 fusion.132
  248.2 0.9 dynamic-slice_bitcast_fusion.14
  250.5 4.1 %fusion.124 = (f32[2,64,64]{2,1,0:T(8,128)S(1)}, f32[2,64,64]{2,1,0:T(8,128)S(1)}, f32[2,64,64]{2,1,0:T(8,128)S(1)}) fusion(f32[2,64,64]{1,2,0:T(8,128)S(1)} %copy.335, f32[2,64,64]{1,2,0:T(8,128)S(1)} %copy.336, f32[2,64,64]{2,1,0:T(8,128)S(1)} %reduce_window_sum.59, f32[2,64,64]{2,1,0:T(8,128)S(1)} %fusion.123, ...), kind=kLoop, calls=%fused_computation.32.clone.1 | loop fusion | flops 5218304 | bytes 233472 | tf_op jit(solution)/shard_map/transpose(jvp())/while/body/eval_jaxpr/checkpoint/reduce_sum | solution.py:38
  255.5 2.0 fusion.131
  257.4 2.0 fusion.132
  261.4 0.9 dynamic-slice_bitcast_fusion.14
  263.7 4.1 %fusion.124 = (f32[2,64,64]{2,1,0:T(8,128)S(1)}, f32[2,64,64]{2,1,0:T(8,128)S(1)}, f32[2,64,64]{2,1,0:T(8,128)S(1)}) fusion(f32[2,64,64]{1,2,0:T(8,128)S(1)} %copy.335, f32[2,64,64]{1,2,0:T(8,128)S(1)} %copy.336, f32[2,64,64]{2,1,0:T(8,128)S(1)} %reduce_window_sum.59, f32[2,64,64]{2,1,0:T(8,128)S(1)} %fusion.123, ...), kind=kLoop, calls=%fused_computation.32.clone.1 | loop fusion | flops 5218304 | bytes 233472 | tf_op jit(solution)/shard_map/transpose(jvp())/while/body/eval_jaxpr/checkpoint/reduce_sum | solution.py:38
  268.6 2.0 fusion.131
  270.6 2.0 fusion.132
  274.8 0.7 copy.214
  275.5 1.0 copy.247
  276.5 0.7 copy.215
  277.2 1.0 copy.212
  278.2 0.8 copy.216
  279.4 0.8 copy.217
  (287 shorter events, 26.3 us)
Async XLA Ops:
  7.2 51.5 %copy-start = (bf16[1,2048,256]{2,1,0:T(8,128)(2,1)S(1)}, bf16[1,2048,256]{2,1,0:T(8,128)(2,1)}, u32[]{:S(2)}) copy-start(bf16[1,2048,256]{2,1,0:T(8,128)(2,1)} %param.25) | copy-start | bytes 3145732
  7.2 51.5 %all-gather.7.cloned.1.call-start = ((), (), s32[]{:S(2)}) async-start(), calls=%async_computation.5 | async-start | bytes 2621440 | tf_op jit(solution)/shard_map/all_gather | solution.py:187
  13.2 24.9 %copy-start.19 = (f32[256,2]{0,1:T(2,128)S(1)}, f32[256,2]{0,1:T(2,128)}, u32[]{:S(2)}) copy-start(f32[256,2]{0,1:T(2,128)} %param.24) | copy-start | bytes 6148
  36.9 45.9 %all-gather.9.cloned.1.call-start = ((), (), s32[]{:S(2)}) async-start(), calls=%async_computation.6 | async-start | bytes 2621440 | tf_op jit(solution)/shard_map/all_gather | solution.py:188
  40.5 20.5 %copy-start.3 = (bf16[1,2048,256]{2,1,0:T(8,128)(2,1)S(1)}, bf16[1,2048,256]{2,1,0:T(8,128)(2,1)}, u32[]{:S(2)}) copy-start(bf16[1,2048,256]{2,1,0:T(8,128)(2,1)} %param.26) | copy-start | bytes 3145732
  58.3 86.2 %reduce-scatter.3.cloned.1.call-start = ((), (), s32[]{:S(2)}) async-start(), calls=%async_computation.7 | async-start | bytes 2621440 | tf_op jit(solution)/shard_map/reduce_scatter | solution.py:193
  61.0 24.5 %copy-start.8 = (f32[512,256]{1,0:T(8,128)}, f32[512,256]{1,0:T(8,128)S(1)}, u32[]{:S(2)}) copy-start(f32[512,256]{1,0:T(8,128)S(1)} %fusion.32) | copy-start | bytes 1572868
  63.5 23.5 %copy-start.10 = (f32[512,256]{1,0:T(8,128)}, f32[512,256]{1,0:T(8,128)S(1)}, u32[]{:S(2)}) copy-start(f32[512,256]{1,0:T(8,128)S(1)} %fusion.35) | copy-start | bytes 1572868
  85.5 0.7 copy-start.12
  85.5 1.5 copy-start.14
  87.0 2.2 copy-start.17
  87.0 2.4 copy-start.15
  87.0 4.2 %copy-start.18 = (bf16[256,128]{1,0:T(8,128)(2,1)S(1)}, bf16[256,128]{1,0:T(8,128)(2,1)}, u32[]{:S(2)}) copy-start(bf16[256,128]{1,0:T(8,128)(2,1)} %param.30) | copy-start | bytes 196612
  89.1 2.4 copy-start.16
  144.5 13.7 %all-to-all-start.2 = ((bf16[8,64,512]{2,1,0:T(8,128)(2,1)}), bf16[8,64,512]{2,1,0:T(8,128)(2,1)S(1)}, u32[]{:S(2)}, u32[]{:S(2)}) async-start(bf16[8,64,512]{2,1,0:T(8,128)(2,1)} %bitcast.335), calls=%async_computation.3 | async-start | bytes 1048576 | tf_op jit(solution)/shard_map/all_to_all | solution.py:196
  148.0 32.3 %all-gather.11.cloned.1.call-start = ((), (), s32[]{:S(2)}) async-start(), calls=%async_computation.8 | async-start | bytes 1310720 | tf_op jit(solution)/shard_map/all_gather | solution.py:199
  163.3 7.9 %copy-start.13 = (bf16[512,256]{1,0:T(8,128)(2,1)S(1)}, bf16[512,256]{1,0:T(8,128)(2,1)}, u32[]{:S(2)}) copy-start(bf16[512,256]{1,0:T(8,128)(2,1)} %copy-done.12) | copy-start | bytes 786436
  165.2 114.9 %reduce-scatter.5.cloned.1.call-start = ((), (), s32[]{:S(2)}) async-start(), calls=%async_computation.9 | async-start | bytes 2359296 | tf_op jit(solution)/shard_map/reduce_scatter | solution.py:203
  170.5 4.1 %copy-start.20 = (bf16[512,2048]{1,0:T(8,128)(2,1)S(1)}, bf16[512,2048]{1,0:T(8,128)(2,1)}, u32[]{:S(2)}) copy-start(bf16[512,2048]{1,0:T(8,128)(2,1)} %all-gather.7.cloned.1.call-done) | copy-start | bytes 6291460
  174.6 2.9 copy-start.2
  174.6 2.9 copy-start.9
  174.6 2.9 copy-start.11
  180.2 3.2 %copy-start.1 = (bf16[256,2048]{1,0:T(8,128)(2,1)S(1)}, bf16[256,2048]{1,0:T(8,128)(2,1)}, u32[]{:S(2)}) copy-start(bf16[256,2048]{1,0:T(8,128)(2,1)} %all-gather.11.cloned.1.call-done) | copy-start | bytes 3145732
  223.2 9.9 %copy-start.4 = (bf16[4,2,64,64]{3,1,2,0:T(2,128)(2,1)S(1)}, bf16[4,2,64,64]{3,1,2,0:T(2,128)(2,1)}, u32[]{:S(2)}) copy-start(bf16[4,2,64,64]{3,1,2,0:T(2,128)(2,1)} %get-tuple-element.1077) | copy-start | bytes 196612 | tf_op jit(solution)/shard_map/transpose(jvp())/while
  223.2 10.2 %copy-start.6 = (bf16[4,2,64,128]{3,2,0,1:T(8,128)(2,1)S(1)}, bf16[4,2,64,128]{3,2,0,1:T(8,128)(2,1)}, u32[]{:S(2)}) copy-start(bf16[4,2,64,128]{3,2,0,1:T(8,128)(2,1)} %get-tuple-element.1078) | copy-start | bytes 393220 | tf_op jit(solution)/shard_map/transpose(jvp())/while
  233.4 0.7 copy-start.5
  233.8 0.7 copy-start.7
  236.4 9.9 %copy-start.4 = (bf16[4,2,64,64]{3,1,2,0:T(2,128)(2,1)S(1)}, bf16[4,2,64,64]{3,1,2,0:T(2,128)(2,1)}, u32[]{:S(2)}) copy-start(bf16[4,2,64,64]{3,1,2,0:T(2,128)(2,1)} %get-tuple-element.1077) | copy-start | bytes 196612 | tf_op jit(solution)/shard_map/transpose(jvp())/while
  236.4 10.2 %copy-start.6 = (bf16[4,2,64,128]{3,2,0,1:T(8,128)(2,1)S(1)}, bf16[4,2,64,128]{3,2,0,1:T(8,128)(2,1)}, u32[]{:S(2)}) copy-start(bf16[4,2,64,128]{3,2,0,1:T(8,128)(2,1)} %get-tuple-element.1078) | copy-start | bytes 393220 | tf_op jit(solution)/shard_map/transpose(jvp())/while
  246.6 0.7 copy-start.5
  246.9 0.7 copy-start.7
  249.5 9.9 %copy-start.4 = (bf16[4,2,64,64]{3,1,2,0:T(2,128)(2,1)S(1)}, bf16[4,2,64,64]{3,1,2,0:T(2,128)(2,1)}, u32[]{:S(2)}) copy-start(bf16[4,2,64,64]{3,1,2,0:T(2,128)(2,1)} %get-tuple-element.1077) | copy-start | bytes 196612 | tf_op jit(solution)/shard_map/transpose(jvp())/while
  249.6 10.2 %copy-start.6 = (bf16[4,2,64,128]{3,2,0,1:T(8,128)(2,1)S(1)}, bf16[4,2,64,128]{3,2,0,1:T(8,128)(2,1)}, u32[]{:S(2)}) copy-start(bf16[4,2,64,128]{3,2,0,1:T(8,128)(2,1)} %get-tuple-element.1078) | copy-start | bytes 393220 | tf_op jit(solution)/shard_map/transpose(jvp())/while
  259.8 0.7 copy-start.5
  260.1 0.7 copy-start.7
  262.7 9.9 %copy-start.4 = (bf16[4,2,64,64]{3,1,2,0:T(2,128)(2,1)S(1)}, bf16[4,2,64,64]{3,1,2,0:T(2,128)(2,1)}, u32[]{:S(2)}) copy-start(bf16[4,2,64,64]{3,1,2,0:T(2,128)(2,1)} %get-tuple-element.1077) | copy-start | bytes 196612 | tf_op jit(solution)/shard_map/transpose(jvp())/while
  262.7 10.2 %copy-start.6 = (bf16[4,2,64,128]{3,2,0,1:T(8,128)(2,1)S(1)}, bf16[4,2,64,128]{3,2,0,1:T(8,128)(2,1)}, u32[]{:S(2)}) copy-start(bf16[4,2,64,128]{3,2,0,1:T(8,128)(2,1)} %get-tuple-element.1078) | copy-start | bytes 393220 | tf_op jit(solution)/shard_map/transpose(jvp())/while
  272.9 0.7 copy-start.5
  273.2 0.7 copy-start.7
Sparse Core Ops, SparseCore 0:
  37.0 21.5 all-gather.6
  60.2 22.5 all-gather.8
  89.3 31.1 reduce-scatter.2
  165.3 14.8 all-gather.10
  184.2 70.5 reduce-scatter.4
where the time goes:
time: 287 us
  blocking collectives  124 us (43%)
  other arithmetic  53.2 us (19%)
  local copies, waits for them, and re-layouts  32.3 us (11%)
  matrix products  31.7 us (11%)
  waiting for transfers between devices  25.1 us (9%)
  between operations  14.4 us (5%)
  starting transfers between devices  3.88 us (1%)
    all_gather x3, blocking collectives, entering(): everything = jax.tree.map(lambda part: lax.all_gather(part, axis), shard)  84.7 us
    all_to_all x1, blocking collectives, shards(): lax.all_to_all(own_input[source_rows], 'sp', split_axis=0, concat_axis=0,...  21.7 us
    all_gather x1, waiting for transfers between devices, shards(): lax.all_gather(arrived[1], 'tp', axis=1, tiled=True)  19.3 us
    all_to_all x1, blocking collectives, shards(): lax.all_to_all(own_scaled[sorting], 'sp', split_axis=0, concat_axis=0, ti...  17.8 us
    reduce_sum x4, other arithmetic, block_step(): difference = cumulative[:, :, None, :] - cumulative[:, None, :, :]  16.3 us
    while x8, other arithmetic  16 us
  transfers between devices with their start and end apart: 6, of which 4 were waited for; matrix products, arithmetic and copies ran while one was open for 32% of the time, Pallas kernels for 0%

commit v1 on v0

--- a/solution.py
+++ b/solution.py
@@ -185,7 +185,7 @@
     )
     routed, routed_cot = (
         lax.all_gather(arrived[0], "tp", axis=1, tiled=True),
-        lax.all_gather(arrived[1], "tp", axis=1, tiled=True),
+        jnp.concatenate(lax.all_gather(arrived[1], "tp"), axis=1),
     )
     grad_gate, grad_up, grad_down, partial_value = expert_pass(
         routed, routed_cot, gate_local, up_local, down_local

time: 287 us -> 290 us (1.010)
  local copies, waits for them, and re-layouts: 32.3 us -> 35.5 us
  transfers between devices with their start and end apart: 6 -> 6, of which waited for: 4 -> 4; matrix products, arithmetic and copies ran while one was open for 32% -> 31% of each run, Pallas kernels for 0% -> 0%
where the time goes in v1:
time: 290 us
  blocking collectives  124 us (43%)
  other arithmetic  53.2 us (18%)
  local copies, waits for them, and re-layouts  35.5 us (12%)
  matrix products  32.4 us (11%)
  waiting for transfers between devices  24.4 us (8%)
  between operations  14.3 us (5%)
  starting transfers between devices  3.88 us (1%)
    all_gather x3, blocking collectives, entering(): everything = jax.tree.map(lambda part: lax.all_gather(part, axis), shard)  84.5 us
    all_to_all x1, blocking collectives, shards(): lax.all_to_all(own_input[source_rows], 'sp', split_axis=0, concat_axis=0,...  21.7 us
    all_gather x1, waiting for transfers between devices, shards(): lax.all_gather(arrived[1], 'tp')  17.9 us
    all_to_all x1, blocking collectives, shards(): lax.all_to_all(own_scaled[sorting], 'sp', split_axis=0, concat_axis=0, ti...  17.8 us
    reduce_sum x4, other arithmetic, block_step(): difference = cumulative[:, :, None, :] - cumulative[:, None, :, :]  16.3 us
    while x8, other arithmetic  16 us
  transfers between devices with their start and end apart: 6, of which 4 were waited for; matrix products, arithmetic and copies ran while one was open for 31% of the time, Pallas kernels for 0%

profile of v1, /device:TPU:0, one launch (start us, length us, event | category | flops | bytes accessed | tf_op | source)
XLA Modules:
  0.0 289.6 jit_solution(11537079997160557225)
XLA Ops:
  7.2 0.9 copy.183
  8.3 3.8 %sort.34 = (s32[512]{0:T(512)}, s32[512]{0:T(512)S(1)}) sort(s32[512]{0:T(512)S(1)} %reshape.177, s32[512]{0:T(512)S(1)} %iota.42), dimensions={0}, to_apply=%region_0.0 | sort | flops 4608 | bytes 8192 | tf_op jit(solution)/shard_map/jit(argsort)/sort | solution.py:168
  12.1 1.1 dynamic-slice_convert_fusion
  13.2 2.0 gather_fusion
  15.2 21.7 %all_to_all.33 = bf16[8,64,512]{2,1,0:T(8,128)(2,1)} all-to-all(bf16[8,64,512]{2,1,0:T(8,128)(2,1)S(1)} %bitcast.318), channel_id=1, replica_groups=mesh['sp'=8,'tp'=4] {'sp'}, dimensions={0} | all-to-all | bytes 1048576 | tf_op jit(solution)/shard_map/all_to_all | solution.py:183
  37.3 0.7 mul.256
  38.5 2.0 gather_fusion.1
  40.5 17.8 %all_to_all.34 = bf16[8,64,512]{2,1,0:T(8,128)(2,1)} all-to-all(bf16[8,64,512]{2,1,0:T(8,128)(2,1)S(1)} %bitcast.319), channel_id=1, replica_groups=mesh['sp'=8,'tp'=4] {'sp'}, dimensions={0} | all-to-all | bytes 1048576 | tf_op jit(solution)/shard_map/all_to_all | solution.py:184
  58.7 3.1 %fusion.32 = f32[512,256]{1,0:T(8,128)} fusion(bf16[512,2048]{1,0:T(8,128)(2,1)} %all-gather.7.cloned.1.call-done, bf16[1,2048,256]{2,1,0:T(8,128)(2,1)S(1)} %copy-done), kind=kOutput, calls=%fused_computation.76 | convolution fusion | flops 536870912 | bytes 3670016 | tf_op jit(solution)/shard_map/dot_general | solution.py:77
  61.8 3.1 %fusion.35 = f32[512,256]{1,0:T(8,128)} fusion(bf16[512,2048]{1,0:T(8,128)(2,1)} %all-gather.7.cloned.1.call-done, bf16[1,2048,256]{2,1,0:T(8,128)(2,1)S(1)} %copy-done.4), kind=kOutput, calls=%fused_computation.79 | convolution fusion | flops 536870912 | bytes 3670016 | tf_op jit(solution)/shard_map/dot_general | solution.py:78
  64.9 17.9 %all-gather.9.cloned.1.call-done = bf16[4,512,512]{2,1,0:T(8,128)(2,1)} async-done(((bf16[1,512,512]{2,1,0:T(8,128)(2,1)}), bf16[4,512,512]{2,1,0:T(8,128)(2,1)}) %all-gather.9.cloned.1.call-update) | async-done | bytes 2097168 | tf_op jit(solution)/shard_map/all_gather | solution.py:188
  82.8 2.8 copy.185
  85.6 3.1 %multiply_convert_fusion.2 = (bf16[512,256]{1,0:T(8,128)(2,1)S(1)}, bf16[512,256]{1,0:T(8,128)(2,1)S(1)}) fusion(f32[512,256]{1,0:T(8,128)} %fusion.32, f32[512,256]{1,0:T(8,128)} %fusion.35, bf16[512,2048]{0,1:T(8,128)(2,1)S(1)} %bitcast.320, bf16[1,256,2048]{2,1,0:T(8,128)(2,1)} %param.27), kind=kOutput, calls=%fused_computation.90 | convolution fusion | flops 538574848 | bytes 4718592 | tf_op jit(solution)/shard_map/dot_general | solution.py:82
  88.7 0.7 fusion.30
  89.5 0.6 copy-done.5
  90.2 2.1 add_convert_fusion
  92.6 1.2 reduce-window.6
  94.8 20.5 %all-gather.1 = f32[16,1,64]{2,1,0:T(1,128)S(1)} all-gather(f32[2,1,64]{2,1,0:T(1,128)S(1)} %bitcast.351), channel_id=3, replica_groups=mesh['sp'=8,'tp'=4] {'sp'}, dimensions={0}, use_global_device_ids=true | all-gather | bytes 4608 | tf_op jit(solution)/shard_map/all_gather | solution.py:14
  116.1 31.6 %all-gather.2 = f32[16,64,128]{2,1,0:T(8,128)S(1)} all-gather(f32[2,64,128]{2,1,0:T(8,128)S(1)} %fusion.43), channel_id=4, replica_groups=mesh['sp'=8,'tp'=4] {'sp'}, dimensions={0}, use_global_device_ids=true | all-gather | bytes 589824 | tf_op jit(solution)/shard_map/all_gather | solution.py:14
  147.6 3.5 %all-to-all-start.2 = ((bf16[8,64,512]{2,1,0:T(8,128)(2,1)}), bf16[8,64,512]{2,1,0:T(8,128)(2,1)S(1)}, u32[]{:S(2)}, u32[]{:S(2)}) async-start(bf16[8,64,512]{2,1,0:T(8,128)(2,1)} %bitcast.340), calls=%async_computation.3 | async-start | bytes 1048576 | tf_op jit(solution)/shard_map/all_to_all | solution.py:196
  151.4 1.1 while.67
  152.6 3.8 %sort.35 = (s32[512]{0:T(512)}, s32[512]{0:T(512)S(1)}) sort(s32[512]{0:T(512)S(1)} %get-tuple-element.514, s32[512]{0:T(512)S(1)} %iota.43), dimensions={0}, to_apply=%region_2.3 | sort | flops 4608 | bytes 8192 | tf_op jit(solution)/shard_map/jit(argsort)/sort | solution.py:170
  156.9 4.4 %all-to-all-done.2 = bf16[8,64,512]{2,1,0:T(8,128)(2,1)S(1)} async-done(((bf16[8,64,512]{2,1,0:T(8,128)(2,1)}), bf16[8,64,512]{2,1,0:T(8,128)(2,1)S(1)}, u32[]{:S(2)}, u32[]{:S(2)}) %all-to-all-start.2) | async-done | bytes 524320 | tf_op jit(solution)/shard_map/all_to_all | solution.py:196
  161.3 2.6 gather_fusion.2
  164.0 1.7 reshape.193
  165.7 0.8 fusion.53
  166.5 1.9 fusion.40
  168.4 5.1 %while.64 = (s32[]{:T(128)}, f32[2,64,128]{2,1,0:T(8,128)S(1)}, f32[4,2,64,128]{3,2,1,0:T(8,128)}, f32[4,2,64,64]{3,2,1,0:T(8,128)S(1)}, f32[4,2,64,64]{2,0,3,1:...) while((s32[]{:T(128)}, f32[2,64,128]{2,1,0:T(8,128)S(1)}, ...), condition=%wide.region_12.13_spmd, body=%wide.region_10.12_spmd.sunk | while | flops 13148162 | bytes 725105 | solution.py:59
  168.4 0.6 bitcast_dynamic-update-slice_fusion.5
  171.0 0.6 bitcast_dynamic-update-slice_fusion.5
  173.7 0.7 broadcast_convert_fusion
  174.4 3.4 %fusion.27 = bf16[1,2048,256]{2,1,0:T(8,128)(2,1)} fusion(bf16[512,2048]{1,0:T(8,128)(2,1)} %all-gather.7.cloned.1.call-done, bf16[512,256]{1,0:T(8,128)(2,1)S(1)} %copy-done.11), kind=kOutput, calls=%fused_computation.70 | convolution fusion | flops 537395200 | bytes 3407872 | tf_op jit(solution)/shard_map/dot_general | solution.py:90
  177.8 1.7 fusion.28
  179.9 1.8 fusion.29
  181.7 1.7 all-gather.11.cloned.1.call-done
  183.4 3.2 %fusion.57 = f32[2048,256]{1,0:T(8,128)} fusion(bf16[256,2048]{1,0:T(8,128)(2,1)} %all-gather.11.cloned.1.call-done, bf16[256,256]{1,0:T(8,128)(2,1)} %param.29), kind=kOutput, calls=%fused_computation.131 | convolution fusion | flops 268435456 | bytes 3276800 | tf_op jit(solution)/shard_map/dot_general | solution.py:204
  186.6 2.4 convolution_convert_fusion.3
  189.0 1.0 copy.194
  190.4 32.5 %all-gather = f32[16,64,128]{2,1,0:T(8,128)S(1)} all-gather(f32[2,64,128]{2,1,0:T(8,128)S(1)} %fusion.45), channel_id=2, replica_groups=mesh['sp'=8,'tp'=4] {'sp'}, dimensions={0}, use_global_device_ids=true | all-gather | bytes 589824 | tf_op jit(solution)/shard_map/all_gather | solution.py:14
  222.8 1.2 while.66
  224.1 0.7 broadcast.54.clone
  224.8 52.6 %while.65 = (s32[]{:T(128)}, f32[2,64,128]{2,1,0:T(8,128)S(1)}, f32[4,2,64,64]{3,1,2,0:T(2,128)S(1)}, bf16[4,2,64,64]{3,1,2,0:T(2,128)(2,1)}, bf16[4,2,64,128]{3...) while((s32[]{:T(128)}, f32[2,64,128]{2,1,0:T(8,128)S(1)}, ...), condition=%wide.region_20.21_spmd, body=%wide.region_13.20_spmd.sunk | while | flops 87216128 | bytes 5496629 | solution.py:59
  224.8 0.9 dynamic-slice_bitcast_fusion.14
  227.1 4.1 %fusion.124 = (f32[2,64,64]{2,1,0:T(8,128)S(1)}, f32[2,64,64]{2,1,0:T(8,128)S(1)}, f32[2,64,64]{2,1,0:T(8,128)S(1)}) fusion(f32[2,64,64]{1,2,0:T(8,128)S(1)} %copy.340, f32[2,64,64]{1,2,0:T(8,128)S(1)} %copy.341, f32[2,64,64]{2,1,0:T(8,128)S(1)} %reduce_window_sum.59, f32[2,64,64]{2,1,0:T(8,128)S(1)} %fusion.123, ...), kind=kLoop, calls=%fused_computation.32.clone.1 | loop fusion | flops 5218304 | bytes 233472 | tf_op jit(solution)/shard_map/transpose(jvp())/while/body/eval_jaxpr/checkpoint/reduce_sum | solution.py:38
  232.1 2.0 fusion.131
  234.1 2.0 fusion.132
  238.0 0.9 dynamic-slice_bitcast_fusion.14
  240.3 4.1 %fusion.124 = (f32[2,64,64]{2,1,0:T(8,128)S(1)}, f32[2,64,64]{2,1,0:T(8,128)S(1)}, f32[2,64,64]{2,1,0:T(8,128)S(1)}) fusion(f32[2,64,64]{1,2,0:T(8,128)S(1)} %copy.340, f32[2,64,64]{1,2,0:T(8,128)S(1)} %copy.341, f32[2,64,64]{2,1,0:T(8,128)S(1)} %reduce_window_sum.59, f32[2,64,64]{2,1,0:T(8,128)S(1)} %fusion.123, ...), kind=kLoop, calls=%fused_computation.32.clone.1 | loop fusion | flops 5218304 | bytes 233472 | tf_op jit(solution)/shard_map/transpose(jvp())/while/body/eval_jaxpr/checkpoint/reduce_sum | solution.py:38
  245.2 2.0 fusion.131
  247.2 2.0 fusion.132
  251.1 0.9 dynamic-slice_bitcast_fusion.14
  253.4 4.1 %fusion.124 = (f32[2,64,64]{2,1,0:T(8,128)S(1)}, f32[2,64,64]{2,1,0:T(8,128)S(1)}, f32[2,64,64]{2,1,0:T(8,128)S(1)}) fusion(f32[2,64,64]{1,2,0:T(8,128)S(1)} %copy.340, f32[2,64,64]{1,2,0:T(8,128)S(1)} %copy.341, f32[2,64,64]{2,1,0:T(8,128)S(1)} %reduce_window_sum.59, f32[2,64,64]{2,1,0:T(8,128)S(1)} %fusion.123, ...), kind=kLoop, calls=%fused_computation.32.clone.1 | loop fusion | flops 5218304 | bytes 233472 | tf_op jit(solution)/shard_map/transpose(jvp())/while/body/eval_jaxpr/checkpoint/reduce_sum | solution.py:38
  258.4 2.0 fusion.131
  260.4 2.0 fusion.132
  264.3 0.9 dynamic-slice_bitcast_fusion.14
  266.6 4.1 %fusion.124 = (f32[2,64,64]{2,1,0:T(8,128)S(1)}, f32[2,64,64]{2,1,0:T(8,128)S(1)}, f32[2,64,64]{2,1,0:T(8,128)S(1)}) fusion(f32[2,64,64]{1,2,0:T(8,128)S(1)} %copy.340, f32[2,64,64]{1,2,0:T(8,128)S(1)} %copy.341, f32[2,64,64]{2,1,0:T(8,128)S(1)} %reduce_window_sum.59, f32[2,64,64]{2,1,0:T(8,128)S(1)} %fusion.123, ...), kind=kLoop, calls=%fused_computation.32.clone.1 | loop fusion | flops 5218304 | bytes 233472 | tf_op jit(solution)/shard_map/transpose(jvp())/while/body/eval_jaxpr/checkpoint/reduce_sum | solution.py:38
  271.6 2.0 fusion.131
  273.5 2.0 fusion.132
  277.7 0.7 copy.219
  278.4 1.0 copy.252
  279.4 0.7 copy.220
  280.2 1.0 copy.217
  281.2 0.8 copy.221
  282.3 0.8 copy.222
  (290 shorter events, 27.3 us)
Async XLA Ops:
  7.2 51.5 %copy-start = (bf16[1,2048,256]{2,1,0:T(8,128)(2,1)S(1)}, bf16[1,2048,256]{2,1,0:T(8,128)(2,1)}, u32[]{:S(2)}) copy-start(bf16[1,2048,256]{2,1,0:T(8,128)(2,1)} %param.25) | copy-start | bytes 3145732
  7.2 51.5 %all-gather.7.cloned.1.call-start = ((), (), s32[]{:S(2)}) async-start(), calls=%async_computation.5 | async-start | bytes 2621440 | tf_op jit(solution)/shard_map/all_gather | solution.py:187
  13.2 24.9 %copy-start.18 = (f32[256,2]{0,1:T(2,128)S(1)}, f32[256,2]{0,1:T(2,128)}, u32[]{:S(2)}) copy-start(f32[256,2]{0,1:T(2,128)} %param.24) | copy-start | bytes 6148
  36.9 45.9 %all-gather.9.cloned.1.call-start = ((), (), s32[]{:S(2)}) async-start(), calls=%async_computation.6 | async-start | bytes 2621440 | tf_op jit(solution)/shard_map/all_gather | solution.py:188
  40.5 21.3 %copy-start.4 = (bf16[1,2048,256]{2,1,0:T(8,128)(2,1)S(1)}, bf16[1,2048,256]{2,1,0:T(8,128)(2,1)}, u32[]{:S(2)}) copy-start(bf16[1,2048,256]{2,1,0:T(8,128)(2,1)} %param.26) | copy-start | bytes 3145732
  58.3 89.3 %reduce-scatter.3.cloned.1.call-start = ((), (), s32[]{:S(2)}) async-start(), calls=%async_computation.7 | async-start | bytes 2621440 | tf_op jit(solution)/shard_map/reduce_scatter | solution.py:193
  85.6 3.9 %copy-start.2 = (bf16[4,512,512]{1,2,0:T(8,128)(2,1)}, bf16[4,512,512]{1,2,0:T(8,128)(2,1)S(1)}, u32[]{:S(2)}) copy-start(bf16[4,512,512]{1,2,0:T(8,128)(2,1)S(1)} %copy.185) | copy-start | bytes 6291460
  88.7 0.8 copy-start.12
  88.7 3.5 %copy-start.10 = (bf16[512,256]{1,0:T(8,128)(2,1)}, bf16[512,256]{1,0:T(8,128)(2,1)S(1)}, u32[]{:S(2)}) copy-start(bf16[512,256]{1,0:T(8,128)(2,1)S(1)} %get-tuple-element.762) | copy-start | bytes 786436
  88.7 1.4 copy-start.5
  90.1 2.1 copy-start.16
  90.1 2.4 copy-start.14
  90.1 4.2 %copy-start.17 = (bf16[256,128]{1,0:T(8,128)(2,1)S(1)}, bf16[256,128]{1,0:T(8,128)(2,1)}, u32[]{:S(2)}) copy-start(bf16[256,128]{1,0:T(8,128)(2,1)} %param.30) | copy-start | bytes 196612
  92.2 2.4 copy-start.15
  147.6 13.7 %all-to-all-start.2 = ((bf16[8,64,512]{2,1,0:T(8,128)(2,1)}), bf16[8,64,512]{2,1,0:T(8,128)(2,1)S(1)}, u32[]{:S(2)}, u32[]{:S(2)}) async-start(bf16[8,64,512]{2,1,0:T(8,128)(2,1)} %bitcast.340), calls=%async_computation.3 | async-start | bytes 1048576 | tf_op jit(solution)/shard_map/all_to_all | solution.py:196
  151.1 32.2 %all-gather.11.cloned.1.call-start = ((), (), s32[]{:S(2)}) async-start(), calls=%async_computation.8 | async-start | bytes 1310720 | tf_op jit(solution)/shard_map/all_gather | solution.py:199
  166.5 7.9 %copy-start.11 = (bf16[512,256]{1,0:T(8,128)(2,1)S(1)}, bf16[512,256]{1,0:T(8,128)(2,1)}, u32[]{:S(2)}) copy-start(bf16[512,256]{1,0:T(8,128)(2,1)} %copy-done.10) | copy-start | bytes 786436
  168.4 114.7 %reduce-scatter.5.cloned.1.call-start = ((), (), s32[]{:S(2)}) async-start(), calls=%async_computation.9 | async-start | bytes 2359296 | tf_op jit(solution)/shard_map/reduce_scatter | solution.py:203
  173.5 4.3 %copy-start.13 = (bf16[512,256]{1,0:T(8,128)(2,1)S(1)}, bf16[512,256]{1,0:T(8,128)(2,1)}, u32[]{:S(2)}) copy-start(bf16[512,256]{1,0:T(8,128)(2,1)} %copy-done.12) | copy-start | bytes 786436
  173.7 4.1 %copy-start.19 = (bf16[512,2048]{1,0:T(8,128)(2,1)S(1)}, bf16[512,2048]{1,0:T(8,128)(2,1)}, u32[]{:S(2)}) copy-start(bf16[512,2048]{1,0:T(8,128)(2,1)} %all-gather.7.cloned.1.call-done) | copy-start | bytes 6291460
  177.7 1.8 copy-start.3
  177.8 1.8 copy-start.20
  177.8 2.2 copy-start.21
  183.4 3.2 %copy-start.1 = (bf16[256,2048]{1,0:T(8,128)(2,1)S(1)}, bf16[256,2048]{1,0:T(8,128)(2,1)}, u32[]{:S(2)}) copy-start(bf16[256,2048]{1,0:T(8,128)(2,1)} %all-gather.11.cloned.1.call-done) | copy-start | bytes 3145732
  226.2 9.9 %copy-start.6 = (bf16[4,2,64,64]{3,1,2,0:T(2,128)(2,1)S(1)}, bf16[4,2,64,64]{3,1,2,0:T(2,128)(2,1)}, u32[]{:S(2)}) copy-start(bf16[4,2,64,64]{3,1,2,0:T(2,128)(2,1)} %get-tuple-element.1077) | copy-start | bytes 196612 | tf_op jit(solution)/shard_map/transpose(jvp())/while
  226.2 10.2 %copy-start.8 = (bf16[4,2,64,128]{3,2,0,1:T(8,128)(2,1)S(1)}, bf16[4,2,64,128]{3,2,0,1:T(8,128)(2,1)}, u32[]{:S(2)}) copy-start(bf16[4,2,64,128]{3,2,0,1:T(8,128)(2,1)} %get-tuple-element.1078) | copy-start | bytes 393220 | tf_op jit(solution)/shard_map/transpose(jvp())/while
  236.4 0.7 copy-start.7
  236.7 0.7 copy-start.9
  239.3 9.9 %copy-start.6 = (bf16[4,2,64,64]{3,1,2,0:T(2,128)(2,1)S(1)}, bf16[4,2,64,64]{3,1,2,0:T(2,128)(2,1)}, u32[]{:S(2)}) copy-start(bf16[4,2,64,64]{3,1,2,0:T(2,128)(2,1)} %get-tuple-element.1077) | copy-start | bytes 196612 | tf_op jit(solution)/shard_map/transpose(jvp())/while
  239.3 10.2 %copy-start.8 = (bf16[4,2,64,128]{3,2,0,1:T(8,128)(2,1)S(1)}, bf16[4,2,64,128]{3,2,0,1:T(8,128)(2,1)}, u32[]{:S(2)}) copy-start(bf16[4,2,64,128]{3,2,0,1:T(8,128)(2,1)} %get-tuple-element.1078) | copy-start | bytes 393220 | tf_op jit(solution)/shard_map/transpose(jvp())/while
  249.5 0.7 copy-start.7
  249.9 0.7 copy-start.9
  252.5 9.9 %copy-start.6 = (bf16[4,2,64,64]{3,1,2,0:T(2,128)(2,1)S(1)}, bf16[4,2,64,64]{3,1,2,0:T(2,128)(2,1)}, u32[]{:S(2)}) copy-start(bf16[4,2,64,64]{3,1,2,0:T(2,128)(2,1)} %get-tuple-element.1077) | copy-start | bytes 196612 | tf_op jit(solution)/shard_map/transpose(jvp())/while
  252.5 10.2 %copy-start.8 = (bf16[4,2,64,128]{3,2,0,1:T(8,128)(2,1)S(1)}, bf16[4,2,64,128]{3,2,0,1:T(8,128)(2,1)}, u32[]{:S(2)}) copy-start(bf16[4,2,64,128]{3,2,0,1:T(8,128)(2,1)} %get-tuple-element.1078) | copy-start | bytes 393220 | tf_op jit(solution)/shard_map/transpose(jvp())/while
  262.7 0.7 copy-start.7
  263.0 0.7 copy-start.9
  265.6 9.9 %copy-start.6 = (bf16[4,2,64,64]{3,1,2,0:T(2,128)(2,1)S(1)}, bf16[4,2,64,64]{3,1,2,0:T(2,128)(2,1)}, u32[]{:S(2)}) copy-start(bf16[4,2,64,64]{3,1,2,0:T(2,128)(2,1)} %get-tuple-element.1077) | copy-start | bytes 196612 | tf_op jit(solution)/shard_map/transpose(jvp())/while
  265.6 10.2 %copy-start.8 = (bf16[4,2,64,128]{3,2,0,1:T(8,128)(2,1)S(1)}, bf16[4,2,64,128]{3,2,0,1:T(8,128)(2,1)}, u32[]{:S(2)}) copy-start(bf16[4,2,64,128]{3,2,0,1:T(8,128)(2,1)} %get-tuple-element.1078) | copy-start | bytes 393220 | tf_op jit(solution)/shard_map/transpose(jvp())/while
  275.8 0.7 copy-start.7
  276.2 0.7 copy-start.9
Sparse Core Ops, SparseCore 0:
  37.0 21.5 all-gather.6
  60.2 22.5 all-gather.8
  92.4 31.1 reduce-scatter.2
  168.5 14.8 all-gather.10
  187.3 70.3 reduce-scatter.4
